TPU v7x, 512 devices: a whole 4x4x16 slice. The times are simulated.
512 devices in a mesh: fs: 16 (over y, x), tp: 32 (over z, core).
Axes of the slice: x: 4, y: 4, z: 16, core: 2. Of those that a mesh axis runs over, the one named last changes fastest.
Arguments:
- saved_inputs: bfloat16 [10752, 4096], P('fs', 'tp'), may hold values from -6 to 6
- proj_cotangent: bfloat16 [10752, 4096], P('fs', 'tp'), may hold values from -0.057861328 to 0.057861328
- saved_hidden: bfloat16 [10752, 4096], P('fs', 'tp'), may hold values from -6 to 6
- out_cotangent: bfloat16 [10752, 4096], P('fs', 'tp'), may hold values from -0.057861328 to 0.057861328
- factors: bfloat16 [2, 4096, 128], replicated, may hold values from -0.46875 to 0.46875
- w_proj: float32 [4096, 4096], P('fs', 'tp'), may hold values from -0.09375 to 0.09375
- w_out: float32 [4096, 4096], P('tp', 'fs'), may hold values from -0.09375 to 0.09375
- moment_first: float32 [2, 128, 4096], P(None, None, 'tp'), may hold values from -1.8 to 1.8
- moment_second: float32 [2, 128, 4096], P(None, None, 'tp'), may hold values from 0.05 to 1
Outputs:
- proj_next: float32 [4096, 4096], P('fs', 'tp')
- out_next: float32 [4096, 4096], P('tp', 'fs')
- proj_copy: bfloat16 [4096, 4096], P(None, 'tp')
- out_copy: bfloat16 [4096, 4096], P('tp')
- first_next: float32 [2, 128, 4096], P(None, None, 'tp')
- second_next: float32 [2, 128, 4096], P(None, None, 'tp')
All inputs are finite; a program needn't handle non-finite values.
Results may differ from a plain program's by a relative error of at most 0.001.
Values may be sent and summed in bfloat16 or wider, within the bound.
No kernel may reach another device: no remote copies, remote signals or barrier semaphores. Data moves between devices by JAX's collectives and lax.ppermute only.
A program may use at most 64 MiB of HBM per device.

v0:
```python
import jax
import jax.numpy as jnp
from jax import lax
from jax.sharding import Mesh
from jax.sharding import PartitionSpec as P

FS = ("fs_0", "fs_1")
TP = ("tp_0", "tp_1")
beta_first = 0.9
beta_second = 0.95
learn_rate = 0.02
epsilon = 1e-06


def split_up(x, dim, count):
    before, after = (x.shape[:dim], x.shape[dim + 1 :])
    return jnp.moveaxis(x.reshape(*before, count, -1, *after), dim, 0)


def sum_at_owner(x, axis, dim):
    count = lax.axis_size(axis)
    blocks = lax.all_to_all(split_up(x, dim, count), axis, 0, 0, tiled=True)
    return jnp.sum(blocks, axis=0)


def rows_for(lines, count):
    spare = -lines.shape[0] % count
    if not spare:
        return lines
    return jnp.concatenate([lines, jnp.zeros((spare, *lines.shape[1:]), lines.dtype)])


def sent_to_all(x, axis):
    count = lax.axis_size(axis)
    return lax.all_to_all(jnp.broadcast_to(x[None], (count, *x.shape)), axis, 0, 0, tiled=True)


def in_order(blocks, dim):
    blocks = jnp.moveaxis(blocks, 0, dim)
    dims = blocks.shape
    return blocks.reshape(*dims[:dim], dims[dim] * dims[dim + 1], *dims[dim + 2 :])


def gather_directly(x, axis, dim):
    blocks = sent_to_all(x, axis)
    return in_order(blocks, dim)


def sum_by_parts(x, axes):
    own = sum_at_owner(rows_for(x, lax.axis_size(axes)), axes, 0)
    whole = gather_directly(own, axes, 0)
    return whole[: len(x)].reshape(x.shape)


def packed_total(arrays, axis):
    ends = [0]
    for a in arrays:
        ends.append(ends[-1] + a.size)
    total = sum_by_parts(jnp.concatenate([a.ravel() for a in arrays]), axis)
    return tuple((total[b:e].reshape(a.shape) for a, b, e in zip(arrays, ends, ends[1:])))


def total_of(x, axes):
    lines = x.reshape(-1, x.shape[-1])
    own = sum_at_owner(rows_for(lines, lax.axis_size(axes)), axes, 0)
    whole = gather_directly(own, axes, 0)
    return whole[: len(lines)].reshape(x.shape)


def of_everyone(x, axis):
    return sent_to_all(x, axis).sum(axis=0)


def one_axis_at_a_time(x, axes):
    far, near = axes
    nearer = of_everyone(x, near)
    return of_everyone(nearer, far)


def gather_turned(arrays, axis, dims):
    turned = [jnp.moveaxis(a, dim, 0) for a, dim in zip(arrays, dims)]
    widths = [t[0].size for t in turned]
    both = jnp.concatenate([t.reshape(-1, w) for t, w in zip(turned, widths)], axis=1)
    result = lax.all_gather(both, axis, axis=0, tiled=True)
    blocks = jnp.split(result, [sum(widths[:k]) for k in range(1, len(widths))], axis=1)
    return tuple(
        (
            jnp.moveaxis(b.reshape(-1, *t.shape[1:]), 0, dim)
            for b, t, dim in zip(blocks, turned, dims)
        )
    )


def over_tokens(left_rows, right_rows, precise):
    return lax.dot_general(
        left_rows,
        right_rows,
        (((0,), (0,)), ((), ())),
        preferred_element_type=jnp.float32,
        precision=precise,
    )


def body(
    saved_inputs,
    proj_cotangent,
    saved_hidden,
    out_cotangent,
    factors,
    w_proj,
    w_out,
    moment_first,
    moment_second,
):
    highest = lax.Precision.HIGHEST
    fs_count = lax.axis_size(FS)
    tp_count = lax.axis_size(TP)
    d_model = factors.shape[1]
    hidden_width = proj_cotangent.shape[1]
    fs_rows = d_model // fs_count
    tp_feats = saved_inputs.shape[1]
    own_rows = lax.dynamic_slice_in_dim(factors, lax.axis_index(FS) * fs_rows, fs_rows, 1).astype(
        jnp.float32
    )
    own_feats = lax.dynamic_slice_in_dim(factors, lax.axis_index(TP) * tp_feats, tp_feats, 1)
    proj_rows = jnp.dot(saved_inputs, own_feats[0], preferred_element_type=jnp.float32)
    out_rows = jnp.dot(out_cotangent, own_feats[1], preferred_element_type=jnp.float32)
    proj_rows, out_rows = packed_total((proj_rows, out_rows), TP)
    partial_sums = jnp.stack(
        [
            over_tokens(proj_rows, proj_cotangent.astype(jnp.float32), highest),
            over_tokens(out_rows, saved_hidden.astype(jnp.float32), highest),
        ]
    )
    small_grads = total_of(partial_sums, FS)
    first_next = beta_first * moment_first + (1.0 - beta_first) * small_grads
    second_next = beta_second * moment_second + (1.0 - beta_second) * small_grads * small_grads
    direction = first_next / (jnp.sqrt(second_next) + epsilon)
    update_full = jnp.einsum("kdr,kre->kde", own_rows, direction, precision=highest)
    squares = one_axis_at_a_time(
        jnp.sum(update_full * update_full, axis=(1, 2)), (("fs_0", "fs_1"), ("tp_0", "tp_1"))
    )
    norm_scale = lax.rsqrt(squares / (d_model * hidden_width * tp_count) + epsilon)
    stepped = update_full * norm_scale[:, None, None]
    proj_next = w_proj - learn_rate * stepped[0]
    out_next = w_out - learn_rate * stepped[1].T
    proj_copy, out_copy = gather_turned(
        (proj_next.astype(jnp.bfloat16), out_next.astype(jnp.bfloat16)), FS, (0, 1)
    )
    return (proj_next, out_next, proj_copy, out_copy, first_next, second_next)


def solution(mesh):
    torus = Mesh(mesh.devices.reshape(4, 4, 16, 2), ("fs_0", "fs_1", "tp_0", "tp_1"))
    return jax.shard_map(
        body,
        mesh=torus,
        in_specs=(
            P(FS, TP),
            P(FS, TP),
            P(FS, TP),
            P(FS, TP),
            P(),
            P(FS, TP),
            P(TP, FS),
            P(None, None, TP),
            P(None, None, TP),
        ),
        out_specs=(
            P(FS, TP),
            P(TP, FS),
            P(None, TP),
            P(TP, None),
            P(None, None, TP),
            P(None, None, TP),
        ),
        check_vma=False,
    )
```

profile of v0, /device:TPU:2, one launch (start us, length us, event | category | flops | bytes accessed | tf_op | source)
XLA Modules:
  0.0 230.2 jit_solution(13127133460400732446)
XLA Ops:
  7.2 0.0 copy-start
  7.2 1.6 copy-done
  8.8 1.1 convolution_bitcast_fusion
  9.9 0.1 concatenate.12
  9.9 1.1 convolution_bitcast_fusion.1
  11.1 0.1 concatenate.11
  11.2 0.5 all_to_all.24
  11.7 56.0 %all_to_all.37 = f32[32,1,5376]{2,1,0:T(1,128)S(1)} all-to-all(f32[32,1,5376]{2,1,0:T(1,128)S(1)} %all_to_all.24), channel_id=1, replica_groups=mesh['fs_0'=4,'fs_1'=4,'tp_0'=16,'tp_1'=2] {'tp_0','tp_1'}, dimensions={0} | all-to-all | bytes 1376256 | tf_op jit(solution)/shard_map/all_to_all | solution.py:22
  67.7 0.0 copy-start.1
  67.7 0.4 reduce_sum.45
  68.1 0.0 copy-start.2
  68.1 0.4 broadcast_in_dim.8
  68.5 44.0 %all_to_all.38 = f32[32,1,5376]{2,1,0:T(1,128)S(1)} all-to-all(f32[32,1,5376]{2,1,0:T(1,128)S(1)} %broadcast_in_dim.8), channel_id=1, replica_groups=mesh['fs_0'=4,'fs_1'=4,'tp_0'=16,'tp_1'=2] {'tp_0','tp_1'}, dimensions={0} | all-to-all | bytes 1376256 | tf_op jit(solution)/shard_map/all_to_all | solution.py:35
  112.5 0.1 fusion.19
  112.6 0.0 copy-start.8
  112.6 0.0 copy-done.1
  112.6 0.5 convolution_bitcast_fusion.3
  113.1 0.0 copy-done.2
  113.1 0.0 copy-start.5
  113.1 0.5 convolution_bitcast_fusion.2
  113.7 13.9 %all_to_all.39 = f32[16,16,128]{2,1,0:T(8,128)S(1)} all-to-all(f32[16,16,128]{2,1,0:T(8,128)S(1)} %bitcast.48), channel_id=1, replica_groups=mesh['fs_0'=4,'fs_1'=4,'tp_0'=16,'tp_1'=2] {'fs_0','fs_1'}, dimensions={0} | all-to-all | bytes 262144 | tf_op jit(solution)/shard_map/all_to_all | solution.py:22
  127.6 0.7 broadcast_in_dim.9
  128.3 4.8 %all-to-all-start.3 = ((f32[16,16,128]{2,1,0:T(8,128)}), f32[16,16,128]{2,1,0:T(8,128)S(1)}, u32[]{:S(2)}, u32[]{:S(2)}) async-start(f32[16,16,128]{2,1,0:T(8,128)} %broadcast_in_dim.9), calls=%async_computation.3 | async-start | bytes 262144 | tf_op jit(solution)/shard_map/all_to_all | solution.py:35
  133.0 6.7 %all-to-all-done.3 = f32[16,16,128]{2,1,0:T(8,128)S(1)} async-done(((f32[16,16,128]{2,1,0:T(8,128)}), f32[16,16,128]{2,1,0:T(8,128)S(1)}, u32[]{:S(2)}, u32[]{:S(2)}) %all-to-all-start.3) | async-done | bytes 131104 | tf_op jit(solution)/shard_map/all_to_all | solution.py:35
  139.8 0.0 copy-done.3
  139.8 0.0 copy-done.4
  139.8 0.0 copy-start.6
  139.8 0.0 copy-start.7
  139.8 0.4 multiply_reduce_fusion
  140.3 15.4 %all_to_all.40 = f32[32,1,2]{2,1,0:T(1,128)S(1)} all-to-all(f32[32,1,2]{2,1,0:T(1,128)S(1)} %broadcast_in_dim.10), channel_id=1, replica_groups=mesh['fs_0'=4,'fs_1'=4,'tp_0'=16,'tp_1'=2] {'tp_0','tp_1'}, dimensions={0} | all-to-all | bytes 512 | tf_op jit(solution)/shard_map/all_to_all | solution.py:35
  155.7 0.1 reduce_sum.48
  155.7 0.6 broadcast_in_dim.11
  156.4 4.7 %all-to-all-start.5 = ((f32[16,1,2]{2,1,0:T(1,128)}), f32[16,1,2]{2,1,0:T(1,128)S(1)}, u32[]{:S(2)}, u32[]{:S(2)}) async-start(f32[16,1,2]{2,1,0:T(1,128)} %broadcast_in_dim.11), calls=%async_computation.5 | async-start | bytes 16384 | tf_op jit(solution)/shard_map/all_to_all | solution.py:35
  161.1 0.0 all-gather.2.cloned.1.call-start
  161.1 0.0 copy-done.8
  161.1 0.1 copy.30
  161.2 6.1 %all-to-all-done.5 = f32[16,1,2]{2,1,0:T(1,128)S(1)} async-done(((f32[16,1,2]{2,1,0:T(1,128)}), f32[16,1,2]{2,1,0:T(1,128)S(1)}, u32[]{:S(2)}, u32[]{:S(2)}) %all-to-all-start.5) | async-done | bytes 160 | tf_op jit(solution)/shard_map/all_to_all | solution.py:35
  167.3 0.1 broadcast_multiply_fusion
  167.4 0.0 copy-done.5
  167.5 0.7 convert_bitcast_fusion
  168.1 0.7 pad_maximum_fusion.2
  168.8 0.0 all-gather.2.cloned.1.call-update
  168.8 0.8 copy.31
  169.6 49.8 %all-gather.2.cloned.1.call-done = bf16[4096,256]{0,1:T(8,128)(2,1)} async-done(((bf16[256,256]{0,1:T(8,128)(2,1)}), bf16[4096,256]{0,1:T(8,128)(2,1)}) %all-gather.2.cloned.1.call-update) | async-done | bytes 2097168 | tf_op jit(solution)/shard_map/all_gather | solution.py:84
  219.3 2.7 %slice_bitcast_fusion = (bf16[128,4096]{1,0:T(8,128)(2,1)}, bf16[4096,128]{0,1:T(8,128)(2,1)S(1)}) fusion(bf16[4096,256]{0,1:T(8,128)(2,1)} %all-gather.2.cloned.1.call-done), kind=kLoop, calls=%fused_computation.4 | loop fusion | bytes 4194304 | tf_op jit(solution)/shard_map/transpose | solution.py:88
  222.0 0.0 copy-done.6
  222.0 0.0 copy-done.7
  222.0 1.3 copy.32
  (10 shorter events, 0.2 us)
Async XLA Ops:
  7.2 1.6 copy-start
  67.7 44.9 %copy-start.1 = (bf16[672,128]{1,0:T(8,128)(2,1)S(1)}, bf16[672,128]{1,0:T(8,128)(2,1)}, u32[]{:S(2)}) copy-start(bf16[672,128]{1,0:T(8,128)(2,1)} %param.10) | copy-start | bytes 516100
  68.1 45.0 %copy-start.2 = (bf16[672,128]{1,0:T(8,128)(2,1)S(1)}, bf16[672,128]{1,0:T(8,128)(2,1)}, u32[]{:S(2)}) copy-start(bf16[672,128]{1,0:T(8,128)(2,1)} %param.11) | copy-start | bytes 516100
  112.5 27.2 %copy-start.3 = (f32[2,128,128]{2,1,0:T(8,128)S(1)}, f32[2,128,128]{2,1,0:T(8,128)}, u32[]{:S(2)}) copy-start(f32[2,128,128]{2,1,0:T(8,128)} %param.17) | copy-start | bytes 393220
  112.5 27.2 %copy-start.4 = (f32[2,128,128]{2,1,0:T(8,128)S(1)}, f32[2,128,128]{2,1,0:T(8,128)}, u32[]{:S(2)}) copy-start(f32[2,128,128]{2,1,0:T(8,128)} %param.16) | copy-start | bytes 393220
  112.6 48.5 %copy-start.8 = (f32[256,128]{1,0:T(8,128)S(1)}, f32[256,128]{1,0:T(8,128)}, u32[]{:S(2)}) copy-start(f32[256,128]{1,0:T(8,128)} %param.14) | copy-start | bytes 393220
  113.1 54.3 %copy-start.5 = (f32[128,256]{1,0:T(8,128)S(1)}, f32[128,256]{1,0:T(8,128)}, u32[]{:S(2)}) copy-start(f32[128,256]{1,0:T(8,128)} %param.15) | copy-start | bytes 393220
  128.3 11.5 %all-to-all-start.3 = ((f32[16,16,128]{2,1,0:T(8,128)}), f32[16,16,128]{2,1,0:T(8,128)S(1)}, u32[]{:S(2)}, u32[]{:S(2)}) async-start(f32[16,16,128]{2,1,0:T(8,128)} %broadcast_in_dim.9), calls=%async_computation.3 | async-start | bytes 262144 | tf_op jit(solution)/shard_map/all_to_all | solution.py:35
  139.8 82.2 %copy-start.6 = (f32[2,128,128]{2,1,0:T(8,128)}, f32[2,128,128]{2,1,0:T(8,128)S(1)}, u32[]{:S(2)}) copy-start(f32[2,128,128]{2,1,0:T(8,128)S(1)} %get-tuple-element.38) | copy-start | bytes 393220
  139.8 82.2 %copy-start.7 = (f32[2,128,128]{2,1,0:T(8,128)}, f32[2,128,128]{2,1,0:T(8,128)S(1)}, u32[]{:S(2)}) copy-start(f32[2,128,128]{2,1,0:T(8,128)S(1)} %get-tuple-element.39) | copy-start | bytes 393220
  156.4 10.9 %all-to-all-start.5 = ((f32[16,1,2]{2,1,0:T(1,128)}), f32[16,1,2]{2,1,0:T(1,128)S(1)}, u32[]{:S(2)}, u32[]{:S(2)}) async-start(f32[16,1,2]{2,1,0:T(1,128)} %broadcast_in_dim.11), calls=%async_computation.5 | async-start | bytes 16384 | tf_op jit(solution)/shard_map/all_to_all | solution.py:35
  161.1 58.3 %all-gather.2.cloned.1.call-start = ((), (), s32[]{:S(2)}) async-start(), calls=%async_computation.6 | async-start | bytes 2228224 | tf_op jit(solution)/shard_map/all_gather | solution.py:84
Sparse Core Ops, SparseCore 0:
  168.9 50.3 all-gather.1
where the time goes:
time: 231 us; the launch traced here: 230 us
  blocking collectives  129 us (56%)
  waiting for transfers between devices  62.5 us (27%)
  between operations  14.2 us (6%)
  starting transfers between devices  9.51 us (4%)
  local copies, waits for them, and re-layouts  8.78 us (4%)
  matrix products  3.67 us (2%)
    all_to_all x2, blocking collectives, sum_at_owner(): blocks = lax.all_to_all(split_up(x, dim, count), axis, 0, 0, tiled=True)  69.9 us
    all_to_all x2, blocking collectives, sent_to_all(): lax.all_to_all(jnp.broadcast_to(x[None], (count, *x.shape)), axis, 0, 0,...  59.4 us
    all_gather x1, waiting for transfers between devices, gather_turned(): result = lax.all_gather(both, axis, axis=0, tiled=True)  49.8 us
    all_to_all x2, waiting for transfers between devices, sent_to_all(): lax.all_to_all(jnp.broadcast_to(x[None], (count, *x.shape)), axis, 0, 0,...  12.8 us
    all_to_all x2, starting transfers between devices, sent_to_all(): lax.all_to_all(jnp.broadcast_to(x[None], (count, *x.shape)), axis, 0, 0,...  9.48 us
  transfers between devices with their start and end apart: 3, of which 3 were waited for; matrix products, arithmetic and copies ran while one was open for 0% of the time, Pallas kernels for 0%

commit v1 on v0

--- a/solution.py
+++ b/solution.py
@@ -81,7 +81,9 @@
     turned = [jnp.moveaxis(a, dim, 0) for a, dim in zip(arrays, dims)]
     widths = [t[0].size for t in turned]
     both = jnp.concatenate([t.reshape(-1, w) for t, w in zip(turned, widths)], axis=1)
-    result = lax.all_gather(both, axis, axis=0, tiled=True)
+    result = jnp.concatenate(
+        lax.all_to_all(jnp.stack([both] * lax.axis_size(axis)), axis, 0, 0), axis=0
+    )
     blocks = jnp.split(result, [sum(widths[:k]) for k in range(1, len(widths))], axis=1)
     return tuple(
         (

time: 231 us -> 205 us (0.89)
  the two profiles are of different devices: /device:TPU:2 before, /device:TPU:32 now
where the time goes in v1:
time: 205 us
  blocking collectives  129 us (63%)
  waiting for transfers between devices  44 us (21%)
  local copies, waits for them, and re-layouts  14.2 us (7%)
  starting transfers between devices  11.4 us (6%)
  matrix products  3.67 us (2%)
    all_to_all x2, blocking collectives, sum_at_owner(): blocks = lax.all_to_all(split_up(x, dim, count), axis, 0, 0, tiled=True)  69.2 us
    all_to_all x2, blocking collectives, sent_to_all(): lax.all_to_all(jnp.broadcast_to(x[None], (count, *x.shape)), axis, 0, 0,...  59.7 us
    all_to_all x1, waiting for transfers between devices, gather_turned(): lax.all_to_all(jnp.stack([both] * lax.axis_size(axis)), axis, 0, 0)  28.8 us
    all_to_all x2, waiting for transfers between devices, sent_to_all(): lax.all_to_all(jnp.broadcast_to(x[None], (count, *x.shape)), axis, 0, 0,...  15.3 us
    all_to_all x2, starting transfers between devices, sent_to_all(): lax.all_to_all(jnp.broadcast_to(x[None], (count, *x.shape)), axis, 0, 0,...  6.98 us
    all_to_all x1, starting transfers between devices, gather_turned(): lax.all_to_all(jnp.stack([both] * lax.axis_size(axis)), axis, 0, 0)  4.44 us
  transfers between devices with their start and end apart: 3, of which 3 were waited for; matrix products, arithmetic and copies ran while one was open for 0% of the time, Pallas kernels for 0%

profile of v1, /device:TPU:32, one launch (start us, length us, event | category | flops | bytes accessed | tf_op | source)
XLA Modules:
  0.0 204.5 jit_solution(13621514391069984315)
XLA Ops:
  0.6 0.0 copy-start
  0.7 1.6 copy-done
  2.2 1.1 convolution_bitcast_fusion
  3.3 0.1 concatenate.12
  3.4 1.1 convolution_bitcast_fusion.1
  4.5 0.1 concatenate.11
  4.7 0.5 all_to_all.27
  5.1 54.4 %all_to_all.42 = f32[32,1,5376]{2,1,0:T(1,128)S(1)} all-to-all(f32[32,1,5376]{2,1,0:T(1,128)S(1)} %all_to_all.27), channel_id=1, replica_groups=mesh['fs_0'=4,'fs_1'=4,'tp_0'=16,'tp_1'=2] {'tp_0','tp_1'}, dimensions={0} | all-to-all | bytes 1376256 | tf_op jit(solution)/shard_map/all_to_all | solution.py:22
  59.6 0.0 copy-start.1
  59.6 0.4 reduce_sum.45
  60.0 0.0 copy-start.2
  60.0 0.4 broadcast_in_dim.8
  60.3 43.6 %all_to_all.43 = f32[32,1,5376]{2,1,0:T(1,128)S(1)} all-to-all(f32[32,1,5376]{2,1,0:T(1,128)S(1)} %broadcast_in_dim.8), channel_id=1, replica_groups=mesh['fs_0'=4,'fs_1'=4,'tp_0'=16,'tp_1'=2] {'tp_0','tp_1'}, dimensions={0} | all-to-all | bytes 1376256 | tf_op jit(solution)/shard_map/all_to_all | solution.py:35
  103.9 0.1 fusion.19
  104.0 0.0 copy-start.8
  104.0 0.0 copy-done.1
  104.0 0.5 convolution_bitcast_fusion.3
  104.5 0.0 copy-done.2
  104.5 0.0 copy-start.5
  104.6 0.5 convolution_bitcast_fusion.2
  105.1 14.8 %all_to_all.44 = f32[16,16,128]{2,1,0:T(8,128)S(1)} all-to-all(f32[16,16,128]{2,1,0:T(8,128)S(1)} %bitcast.50), channel_id=1, replica_groups=mesh['fs_0'=4,'fs_1'=4,'tp_0'=16,'tp_1'=2] {'fs_0','fs_1'}, dimensions={0} | all-to-all | bytes 262144 | tf_op jit(solution)/shard_map/all_to_all | solution.py:22
  120.0 0.7 broadcast_in_dim.9
  120.6 3.5 %all-to-all-start.3 = ((f32[16,16,128]{2,1,0:T(8,128)}), f32[16,16,128]{2,1,0:T(8,128)S(1)}, u32[]{:S(2)}, u32[]{:S(2)}) async-start(f32[16,16,128]{2,1,0:T(8,128)} %broadcast_in_dim.9), calls=%async_computation.3 | async-start | bytes 262144 | tf_op jit(solution)/shard_map/all_to_all | solution.py:35
  124.2 7.9 %all-to-all-done.3 = f32[16,16,128]{2,1,0:T(8,128)S(1)} async-done(((f32[16,16,128]{2,1,0:T(8,128)}), f32[16,16,128]{2,1,0:T(8,128)S(1)}, u32[]{:S(2)}, u32[]{:S(2)}) %all-to-all-start.3) | async-done | bytes 131104 | tf_op jit(solution)/shard_map/all_to_all | solution.py:35
  132.1 0.0 copy-done.3
  132.1 0.0 copy-done.4
  132.1 0.0 copy-start.6
  132.2 0.0 copy-start.7
  132.2 0.4 multiply_reduce_fusion
  132.6 16.1 %all_to_all.45 = f32[32,1,2]{2,1,0:T(1,128)S(1)} all-to-all(f32[32,1,2]{2,1,0:T(1,128)S(1)} %broadcast_in_dim.10), channel_id=1, replica_groups=mesh['fs_0'=4,'fs_1'=4,'tp_0'=16,'tp_1'=2] {'tp_0','tp_1'}, dimensions={0} | all-to-all | bytes 512 | tf_op jit(solution)/shard_map/all_to_all | solution.py:35
  148.8 0.1 reduce_sum.48
  148.8 0.6 broadcast_in_dim.11
  149.4 3.5 %all-to-all-start.5 = ((f32[16,1,2]{2,1,0:T(1,128)}), f32[16,1,2]{2,1,0:T(1,128)S(1)}, u32[]{:S(2)}, u32[]{:S(2)}) async-start(f32[16,1,2]{2,1,0:T(1,128)} %broadcast_in_dim.11), calls=%async_computation.5 | async-start | bytes 16384 | tf_op jit(solution)/shard_map/all_to_all | solution.py:35
  152.9 0.0 copy-done.8
  152.9 0.1 copy.36
  153.0 7.3 %all-to-all-done.5 = f32[16,1,2]{2,1,0:T(1,128)S(1)} async-done(((f32[16,1,2]{2,1,0:T(1,128)}), f32[16,1,2]{2,1,0:T(1,128)S(1)}, u32[]{:S(2)}, u32[]{:S(2)}) %all-to-all-start.5) | async-done | bytes 160 | tf_op jit(solution)/shard_map/all_to_all | solution.py:35
  160.4 0.1 broadcast_multiply_fusion
  160.5 0.0 copy-done.5
  160.5 0.7 convert_bitcast_fusion
  161.2 1.5 stack.11
  162.7 0.0 copy-done.6
  162.7 0.0 copy-done.7
  162.7 4.4 %all-to-all-start.6 = ((bf16[16,256,256]{1,2,0:T(8,128)(2,1)}), bf16[16,256,256]{1,2,0:T(8,128)(2,1)}, u32[]{:S(2)}, u32[]{:S(2)}) async-start(bf16[16,256,256]{1,2,0:T(8,128)(2,1)} %stack.11), calls=%async_computation.6 | async-start | bytes 4194304 | tf_op jit(solution)/shard_map/all_to_all | solution.py:85
  167.2 0.8 copy.38
  167.9 28.8 %all-to-all-done.6 = bf16[16,256,256]{1,2,0:T(8,128)(2,1)} async-done(((bf16[16,256,256]{1,2,0:T(8,128)(2,1)}), bf16[16,256,256]{1,2,0:T(8,128)(2,1)}, u32[]{:S(2)}, u32[]{:S(2)}) %all-to-all-start.6) | async-done | bytes 2097184 | tf_op jit(solution)/shard_map/all_to_all | solution.py:85
  196.7 3.9 %copy.37 = bf16[16,256,256]{2,1,0:T(8,128)(2,1)} copy(bf16[16,256,256]{1,2,0:T(8,128)(2,1)} %all-to-all-done.6) | data formatting | bytes 4194304 | tf_op jit(solution)/shard_map/all_to_all | solution.py:85
  200.6 2.6 %slice_bitcast_fusion = (bf16[128,4096]{0,1:T(8,128)(2,1)S(1)}, bf16[4096,128]{1,0:T(8,128)(2,1)}) fusion(bf16[4096,256]{1,0:T(8,128)(2,1)} %bitcast.46), kind=kLoop, calls=%fused_computation.4 | loop fusion | bytes 4194304 | tf_op jit(solution)/shard_map/transpose | solution.py:90
  203.2 1.3 copy.39
  (11 shorter events, 0.2 us)
Async XLA Ops:
  0.6 1.6 copy-start
  59.6 44.5 %copy-start.1 = (bf16[672,128]{1,0:T(8,128)(2,1)S(1)}, bf16[672,128]{1,0:T(8,128)(2,1)}, u32[]{:S(2)}) copy-start(bf16[672,128]{1,0:T(8,128)(2,1)} %param.10) | copy-start | bytes 516100
  60.0 44.6 %copy-start.2 = (bf16[672,128]{1,0:T(8,128)(2,1)S(1)}, bf16[672,128]{1,0:T(8,128)(2,1)}, u32[]{:S(2)}) copy-start(bf16[672,128]{1,0:T(8,128)(2,1)} %param.11) | copy-start | bytes 516100
  103.9 28.2 %copy-start.3 = (f32[2,128,128]{2,1,0:T(8,128)S(1)}, f32[2,128,128]{2,1,0:T(8,128)}, u32[]{:S(2)}) copy-start(f32[2,128,128]{2,1,0:T(8,128)} %param.17) | copy-start | bytes 393220
  103.9 28.2 %copy-start.4 = (f32[2,128,128]{2,1,0:T(8,128)S(1)}, f32[2,128,128]{2,1,0:T(8,128)}, u32[]{:S(2)}) copy-start(f32[2,128,128]{2,1,0:T(8,128)} %param.16) | copy-start | bytes 393220
  104.0 48.9 %copy-start.8 = (f32[256,128]{1,0:T(8,128)S(1)}, f32[256,128]{1,0:T(8,128)}, u32[]{:S(2)}) copy-start(f32[256,128]{1,0:T(8,128)} %param.14) | copy-start | bytes 393220
  104.5 56.0 %copy-start.5 = (f32[128,256]{1,0:T(8,128)S(1)}, f32[128,256]{1,0:T(8,128)}, u32[]{:S(2)}) copy-start(f32[128,256]{1,0:T(8,128)} %param.15) | copy-start | bytes 393220
  120.6 11.5 %all-to-all-start.3 = ((f32[16,16,128]{2,1,0:T(8,128)}), f32[16,16,128]{2,1,0:T(8,128)S(1)}, u32[]{:S(2)}, u32[]{:S(2)}) async-start(f32[16,16,128]{2,1,0:T(8,128)} %broadcast_in_dim.9), calls=%async_computation.3 | async-start | bytes 262144 | tf_op jit(solution)/shard_map/all_to_all | solution.py:35
  132.1 30.6 %copy-start.6 = (f32[2,128,128]{2,1,0:T(8,128)}, f32[2,128,128]{2,1,0:T(8,128)S(1)}, u32[]{:S(2)}) copy-start(f32[2,128,128]{2,1,0:T(8,128)S(1)} %get-tuple-element.44) | copy-start | bytes 393220
  132.2 30.6 %copy-start.7 = (f32[2,128,128]{2,1,0:T(8,128)}, f32[2,128,128]{2,1,0:T(8,128)S(1)}, u32[]{:S(2)}) copy-start(f32[2,128,128]{2,1,0:T(8,128)S(1)} %get-tuple-element.45) | copy-start | bytes 393220
  149.4 10.9 %all-to-all-start.5 = ((f32[16,1,2]{2,1,0:T(1,128)}), f32[16,1,2]{2,1,0:T(1,128)S(1)}, u32[]{:S(2)}, u32[]{:S(2)}) async-start(f32[16,1,2]{2,1,0:T(1,128)} %broadcast_in_dim.11), calls=%async_computation.5 | async-start | bytes 16384 | tf_op jit(solution)/shard_map/all_to_all | solution.py:35
  162.7 34.0 %all-to-all-start.6 = ((bf16[16,256,256]{1,2,0:T(8,128)(2,1)}), bf16[16,256,256]{1,2,0:T(8,128)(2,1)}, u32[]{:S(2)}, u32[]{:S(2)}) async-start(bf16[16,256,256]{1,2,0:T(8,128)(2,1)} %stack.11), calls=%async_computation.6 | async-start | bytes 4194304 | tf_op jit(solution)/shard_map/all_to_all | solution.py:85
